TPU v7x, 512 devices: a whole 4x8x8 slice. The times are simulated.
512 devices in a mesh: sp: 32 (over z, x), tp: 16 (over y, core).
Axes of the slice: x: 4, y: 8, z: 8, core: 2. Of those that a mesh axis runs over, the one named last changes fastest.
Arguments:
- queries: bfloat16 [8192, 2048], P('sp', 'tp'), may hold values from -6 to 6
- keys: bfloat16 [8192, 1024], P('sp', 'tp'), may hold values from -6 to 6
- values: bfloat16 [8192, 1024], P('sp', 'tp'), may hold values from -6 to 6
- docs: int32 [8192], P('sp'), may hold values from 0 to 2, never falling along the last dimension, each value on 1 to 5120 neighbouring positions
- query_gain: float32 [64], replicated, may hold values from 0.5 to 8
- key_gain: float32 [64], replicated, may hold values from 0.5 to 8
- out_weight: bfloat16 [2048, 2048], P('tp'), may hold values from -0.125 to 0.125
- residual: bfloat16 [8192, 2048], P('sp', 'tp'), may hold values from -12 to 12
- norm_gain: float32 [2048], P('tp'), may hold values from 0.1 to 1.9
- routes: int32 [8192, 2], P('sp'), may hold values from 0 to 31, all different within a row; in each aligned block of 256 rows (0 to 255, 256 to 511, ...) at most 20 rows name the same one
- route_weight: float32 [8192, 2], P('sp'), may hold values from 0.1 to 1
- gate_weight: bfloat16 [32, 2048, 4096], P('sp', None, 'tp'), may hold values from -0.3125 to 0.3125
- up_weight: bfloat16 [32, 2048, 4096], P('sp', None, 'tp'), may hold values from -0.3125 to 0.3125
- down_weight: bfloat16 [32, 4096, 2048], P('sp', 'tp'), may hold values from -0.09375 to 0.09375
Outputs:
- mixed: bfloat16 [8192, 2048], P('sp', 'tp')
Inputs may be any that keep to these rules, and one draw needn't show every extreme that they name: `routes`: in each aligned block of 256 rows no expert is named by more than 20 rows, and 20 is reached in some block; a row names 2 different experts. `docs`: document numbers never fall along the sequence; a document holds at most 5120 positions.
All inputs are finite; a program needn't handle non-finite values.
Results may differ from a plain program's by a relative error of at most 0.028.
The roundings to bfloat16 on the way count: a program that leaves them out, or rounds other values in their place, can miss the bound.
Values may be sent and summed in bfloat16 or wider, within the bound.
No kernel may reach another device: no remote copies, remote signals or barrier semaphores. Data moves between devices by JAX's collectives and lax.ppermute only.
A program may use at most 64 MiB of HBM per device.

v0:
```python
import jax
import jax.numpy as jnp
from jax import lax
from jax.sharding import PartitionSpec as P

GRID_W = 64
EPSILON = 1e-06
NEG_BIG = -1e30
ROTARY_BASE = 10000.0
CLAMP_LIMIT = 7.0
SIGMOID_SCALE = 1.702


def sent_together(arrays, axis, dim, along):
    columns = [a.reshape(*a.shape[:along], -1) for a in arrays]
    both = jnp.concatenate(columns, axis=along)
    out, at, gathered = (lax.all_gather(both, axis, axis=dim, tiled=True), 0, [])
    for a, column in zip(arrays, columns):
        piece = out[..., at : at + column.shape[along]]
        gathered.append(piece.reshape(*piece.shape[:along], *a.shape[along:]))
        at += column.shape[along]
    return tuple(gathered)


def cut_along(value, dim, length):
    before, after = (value.shape[:dim], value.shape[dim + 1 :])
    return jnp.moveaxis(value.reshape(*before, length, -1, *after), dim, 0)


def summed_on_arrival(value, axis, dim):
    length = lax.axis_size(axis)
    tiles = lax.all_to_all(cut_along(value, dim, length), axis, 0, 0, tiled=True)
    return jnp.sum(tiles.astype(jnp.float32), axis=0)


def copy_for_each(value, axis):
    length = lax.axis_size(axis)
    return lax.all_to_all(
        jnp.broadcast_to(value[None], (length, *value.shape)), axis, 0, 0, tiled=True
    )


def of_everyone(value, axis):
    everything = copy_for_each(value, axis)
    return jnp.sum(everything, axis=0)


def rope_tables(positions, head_dim):
    quarter = head_dim // 4
    freqs = ROTARY_BASE ** (-jnp.arange(quarter, dtype=jnp.float32) / quarter)
    row_pos = (positions // GRID_W).astype(jnp.float32)
    col_pos = (positions % GRID_W).astype(jnp.float32)
    angle = jnp.concatenate([row_pos[:, None] * freqs, col_pos[:, None] * freqs], axis=1)
    return (jnp.cos(angle), jnp.sin(angle))


def norm_rotate(heads, gain, cosine_table, sine_table):
    entries = heads.astype(jnp.float32)
    entries = (
        entries * lax.rsqrt(jnp.mean(entries * entries, axis=-1, keepdims=True) + EPSILON) * gain
    )
    pairs = entries.reshape(entries.shape[:-1] + (entries.shape[-1] // 2, 2))
    first = pairs[..., 0]
    second = pairs[..., 1]
    cos_rows = cosine_table[:, None, :]
    sin_rows = sine_table[:, None, :]
    turned = jnp.stack(
        [first * cos_rows - second * sin_rows, first * sin_rows + second * cos_rows], axis=-1
    )
    return turned.reshape(heads.shape).astype(jnp.bfloat16)


def clamped_unit(gate_pre, up_pre):
    bounded = jnp.minimum(gate_pre, CLAMP_LIMIT)
    linear = jnp.clip(up_pre, -CLAMP_LIMIT, CLAMP_LIMIT)
    return (bounded * jax.nn.sigmoid(SIGMOID_SCALE * bounded) * (linear + 1.0)).astype(jnp.bfloat16)


def block_length(length):
    block_size = length
    while block_size > 2048 and block_size % 2 == 0:
        block_size = block_size // 2
    return block_size


def softmax_update(running, inputs, query_rot, own_tags, score_scale):
    row_peak, denominator, carried = running
    key_block, value_block, tag_block = inputs
    scores = (
        jnp.einsum("tkgd,pkd->tkgp", query_rot, key_block, preferred_element_type=jnp.float32)
        * score_scale
    )
    allowed = own_tags[:, None, None, None] == tag_block[None, None, None, :]
    scores = jnp.where(allowed, scores, NEG_BIG)
    new_peak = jnp.maximum(row_peak, jnp.max(scores, axis=-1))
    weights = jnp.where(allowed, jnp.exp(scores - new_peak[..., None]), 0.0)
    factor = jnp.exp(row_peak - new_peak)
    denominator = denominator * factor + jnp.sum(weights, axis=-1)
    carried = carried * factor[..., None] + jnp.einsum(
        "tkgp,pkd->tkgd",
        weights.astype(jnp.bfloat16),
        value_block,
        preferred_element_type=jnp.float32,
    )
    return (new_peak, denominator, carried)


def per_device(
    queries,
    keys,
    values,
    docs,
    query_gain,
    key_gain,
    out_weight,
    residual,
    norm_gain,
    routes,
    route_weight,
    gate_weight,
    up_weight,
    down_weight,
):
    tokens = queries.shape[0]
    head_dim = query_gain.shape[0]
    query_heads = queries.shape[1] // head_dim
    pair_heads = keys.shape[1] // head_dim
    pair_width = keys.shape[1]
    positions = lax.axis_index("sp") * tokens + jnp.arange(tokens, dtype=jnp.int32)
    cosine_table, sine_table = rope_tables(positions, head_dim)
    query_rot = norm_rotate(
        queries.reshape(tokens, query_heads, head_dim), query_gain, cosine_table, sine_table
    )
    query_rot = query_rot.reshape(tokens, pair_heads, 2, head_dim)
    key_rot = norm_rotate(
        keys.reshape(tokens, pair_heads, head_dim), key_gain, cosine_table, sine_table
    )
    stacked = jnp.concatenate([key_rot.reshape(tokens, pair_width), values], axis=1)
    own_tags = docs.astype(jnp.bfloat16)
    score_scale = head_dim ** (-0.5)
    stat_shape = (tokens, pair_heads, 2)
    initial = (
        jnp.full(stat_shape, NEG_BIG, jnp.float32),
        jnp.zeros(stat_shape, jnp.float32),
        jnp.zeros(stat_shape + (head_dim,), jnp.float32),
    )
    pair_rows, tag_rows = sent_together((stacked, own_tags), "sp", 0, 1)
    length = pair_rows.shape[0]
    block_size = block_length(length)
    blocks = length // block_size
    key_part = pair_rows[:, :pair_width].reshape(blocks, block_size, pair_heads, head_dim)
    value_part = pair_rows[:, pair_width:].reshape(blocks, block_size, pair_heads, head_dim)
    tag_part = tag_rows.reshape(blocks, block_size)

    def advance(carry_state, inputs):
        return (softmax_update(carry_state, inputs, query_rot, own_tags, score_scale), None)

    result, _ = lax.scan(advance, initial, (key_part, value_part, tag_part))
    row_peak, denominator, carried = result
    attended = (
        (carried / denominator[..., None])
        .astype(jnp.bfloat16)
        .reshape(tokens, query_heads * head_dim)
    )
    width_local = residual.shape[1]
    projected = summed_on_arrival(
        lax.dot_general(
            out_weight, attended, (((0,), (1,)), ((), ())), preferred_element_type=jnp.float32
        ).astype(jnp.bfloat16),
        "tp",
        0,
    )
    mixed_first = residual.astype(jnp.float32) + projected.T
    squares = of_everyone(jnp.sum(mixed_first * mixed_first, axis=1), "tp")
    full_width = width_local * lax.axis_size("tp")
    normed = (mixed_first * lax.rsqrt(squares / full_width + EPSILON)[:, None] * norm_gain).astype(
        jnp.bfloat16
    )
    experts = lax.axis_size("sp")
    top_count = routes.shape[1]
    capacity = max(2, 5 * tokens * top_count // (4 * experts))
    flat_routes = routes.reshape(-1)
    entries = flat_routes.shape[0]
    expert_ids = jnp.arange(experts, dtype=jnp.int32)
    onehot = (flat_routes[:, None] == expert_ids[None, :]).astype(jnp.int32)
    earlier = jnp.cumsum(onehot, axis=0) - onehot
    slot_index = jnp.sum(earlier * onehot, axis=1)
    slot_ids = jnp.arange(capacity, dtype=jnp.int32)
    matches = (flat_routes[:, None, None] == expert_ids[None, :, None]) & (
        slot_index[:, None, None] == slot_ids[None, None, :]
    )
    entry_ids = jnp.arange(entries, dtype=jnp.int32)
    source_entry = jnp.sum(jnp.where(matches, entry_ids[:, None, None], 0), axis=0)
    occupied = jnp.any(matches, axis=0)
    source_row = source_entry // top_count
    gate_local = gate_weight[0]
    up_local = up_weight[0]
    down_local = down_weight[0]
    model_width = gate_local.shape[0]
    outgoing = jnp.where(occupied[..., None], normed[source_row], jnp.zeros((), jnp.bfloat16))
    arrived = lax.all_to_all(outgoing, "sp", split_axis=0, concat_axis=0, tiled=True)
    sources = arrived.shape[0]
    flat_rows = arrived.reshape(-1, width_local)
    column_piece = lax.all_gather(flat_rows, "tp", axis=1, tiled=True)
    gate_pre = jnp.dot(column_piece, gate_local, preferred_element_type=jnp.float32)
    up_pre = jnp.dot(column_piece, up_local, preferred_element_type=jnp.float32)
    hidden = clamped_unit(gate_pre, up_pre)
    partial_value = jnp.dot(hidden, down_local, preferred_element_type=jnp.float32).reshape(
        sources, capacity, model_width
    )
    expert_out = summed_on_arrival(partial_value.astype(jnp.bfloat16), "tp", 2).astype(jnp.bfloat16)
    returned = lax.all_to_all(expert_out, "sp", split_axis=0, concat_axis=0, tiled=True)
    lookup = flat_routes * capacity + slot_index
    picked = (
        returned.reshape(-1, width_local)[lookup]
        .reshape(tokens, top_count, width_local)
        .astype(jnp.float32)
    )
    routed = jnp.sum(route_weight[:, :, None] * picked, axis=1)
    return (mixed_first + routed).astype(jnp.bfloat16)


def solution(mesh):
    in_specs = (
        P("sp", "tp"),
        P("sp", "tp"),
        P("sp", "tp"),
        P("sp"),
        P(),
        P(),
        P("tp", None),
        P("sp", "tp"),
        P("tp"),
        P("sp", None),
        P("sp", None),
        P("sp", None, "tp"),
        P("sp", None, "tp"),
        P("sp", "tp", None),
    )
    out_specs = P("sp", "tp")
    return jax.shard_map(
        per_device, mesh=mesh, in_specs=in_specs, out_specs=out_specs, check_vma=False
    )
```

profile of v0, /device:TPU:24, one launch (start us, length us, event | category | flops | bytes accessed | tf_op | source)
XLA Modules:
  0.0 353.9 jit_solution(10780892546366876018)
XLA Ops:
  6.6 0.9 fusion.36
  7.5 0.8 fusion.37
  8.7 0.7 convert_element_type.95
  9.4 1.4 pad_maximum_fusion
  10.8 0.9 copy.93
  11.8 0.8 mul.256
  12.9 0.2 subtract_convert_fusion
  13.1 0.2 pad_maximum_fusion.1
  13.3 83.1 %all-gather.3.cloned.1.call-done = bf16[8192,129]{0,1:T(8,128)(2,1)} async-done(((bf16[256,129]{0,1:T(8,128)(2,1)}), bf16[8192,129]{0,1:T(8,128)(2,1)}) %all-gather.3.cloned.1.call-update) | async-done | bytes 2113552 | tf_op jit(solution)/shard_map/all_gather | solution.py:17
  96.4 2.7 fusion.54
  99.1 1.8 reshape.581
  100.9 1.6 copy.94
  102.5 0.8 reshape.582
  103.3 1.6 copy.95
  104.9 1.0 slice_reduce_fusion.1
  105.9 35.0 %while.15 = (s32[]{:T(128)}, f32[256,1,2]{0,2,1:T(2,128)S(1)}, f32[256,1,2]{0,2,1:T(2,128)S(1)}, f32[256,1,2,64]{0,3,2,1:T(8,128)S(1)}, bf16[256]{0:T(256)(128)(...) while((s32[]{:T(128)}, f32[256,1,2]{0,2,1:T(2,128)S(1)}, ...), condition=%wide.region_5.6_spmd.clone, body=%wide.region_2.5_spmd.clone.sunk | while | flops 282692608 | bytes 32355992 | solution.py:158
  105.9 0.4 broadcast_compare_fusion.3
  106.3 3.6 %fusion.68 = (f32[256,2]{0,1:T(2,128)S(1)}, f32[2048,256,2]{1,0,2:T(8,128)}) fusion(pred[256,2048]{0,1:T(8,128)(4,1)S(1)} %broadcast_compare_fusion.3, bf16[256,1,2,64]{0,3,2,1:T(8,128)(2,1)S(1)} %get-tuple-element.262, bf16[4,2048,1,64]{1,3,2,0:T(8,128)(2,1)} %get-tuple-element.261, s32[]{:T(128)} %get-tuple-element.244), kind=kOutput, calls=%fused_computation.4.clone.1 | convolution fusion | flops 137362944 | bytes 5048832 | tf_op jit(solution)/shard_map/while/body/eval_jaxpr/tkgd,pkd->tkgp/dot_general | solution.py:90
  110.0 3.5 fusion.71
  113.5 1.1 fusion.70
  114.7 0.4 broadcast_compare_fusion.3
  115.1 3.6 %fusion.68 = (f32[256,2]{0,1:T(2,128)S(1)}, f32[2048,256,2]{1,0,2:T(8,128)}) fusion(pred[256,2048]{0,1:T(8,128)(4,1)S(1)} %broadcast_compare_fusion.3, bf16[256,1,2,64]{0,3,2,1:T(8,128)(2,1)S(1)} %get-tuple-element.262, bf16[4,2048,1,64]{1,3,2,0:T(8,128)(2,1)} %get-tuple-element.261, s32[]{:T(128)} %get-tuple-element.244), kind=kOutput, calls=%fused_computation.4.clone.1 | convolution fusion | flops 137362944 | bytes 5048832 | tf_op jit(solution)/shard_map/while/body/eval_jaxpr/tkgd,pkd->tkgp/dot_general | solution.py:90
  118.7 3.5 fusion.71
  122.2 1.1 fusion.70
  123.4 0.4 broadcast_compare_fusion.3
  123.8 3.6 %fusion.68 = (f32[256,2]{0,1:T(2,128)S(1)}, f32[2048,256,2]{1,0,2:T(8,128)}) fusion(pred[256,2048]{0,1:T(8,128)(4,1)S(1)} %broadcast_compare_fusion.3, bf16[256,1,2,64]{0,3,2,1:T(8,128)(2,1)S(1)} %get-tuple-element.262, bf16[4,2048,1,64]{1,3,2,0:T(8,128)(2,1)} %get-tuple-element.261, s32[]{:T(128)} %get-tuple-element.244), kind=kOutput, calls=%fused_computation.4.clone.1 | convolution fusion | flops 137362944 | bytes 5048832 | tf_op jit(solution)/shard_map/while/body/eval_jaxpr/tkgd,pkd->tkgp/dot_general | solution.py:90
  127.5 3.5 fusion.71
  131.0 1.1 fusion.70
  132.2 0.4 broadcast_compare_fusion.3
  132.6 3.6 %fusion.68 = (f32[256,2]{0,1:T(2,128)S(1)}, f32[2048,256,2]{1,0,2:T(8,128)}) fusion(pred[256,2048]{0,1:T(8,128)(4,1)S(1)} %broadcast_compare_fusion.3, bf16[256,1,2,64]{0,3,2,1:T(8,128)(2,1)S(1)} %get-tuple-element.262, bf16[4,2048,1,64]{1,3,2,0:T(8,128)(2,1)} %get-tuple-element.261, s32[]{:T(128)} %get-tuple-element.244), kind=kOutput, calls=%fused_computation.4.clone.1 | convolution fusion | flops 137362944 | bytes 5048832 | tf_op jit(solution)/shard_map/while/body/eval_jaxpr/tkgd,pkd->tkgp/dot_general | solution.py:90
  136.2 3.5 fusion.71
  139.7 1.1 fusion.70
  141.0 0.5 fusion.26
  141.4 1.3 copy.127
  142.7 7.4 %all-to-all-start = ((bf16[16,128,256]{1,2,0:T(8,128)(2,1)}), bf16[16,128,256]{1,2,0:T(8,128)(2,1)S(1)}, u32[]{:S(2)}, u32[]{:S(2)}) async-start(bf16[16,128,256]{1,2,0:T(8,128)(2,1)} %bitcast.153), calls=%async_computation | async-start | bytes 2097152 | tf_op jit(solution)/shard_map/all_to_all | solution.py:32
  150.2 0.1 eq.81
  150.5 1.2 reduce-window.6
  151.7 0.2 slice_reduce_fusion
  152.1 0.4 fusion.27
  152.8 0.4 and_reduce_fusion
  153.2 23.1 %all-to-all-done = bf16[16,128,256]{1,2,0:T(8,128)(2,1)S(1)} async-done(((bf16[16,128,256]{1,2,0:T(8,128)(2,1)}), bf16[16,128,256]{1,2,0:T(8,128)(2,1)S(1)}, u32[]{:S(2)}, u32[]{:S(2)}) %all-to-all-start) | async-done | bytes 1048608 | tf_op jit(solution)/shard_map/all_to_all | solution.py:32
  176.3 0.1 convert_reduce_fusion
  176.5 0.6 broadcast_in_dim.54
  177.2 5.2 %all-to-all-start.1 = ((f32[16,1,256]{2,1,0:T(1,128)}), f32[16,1,256]{2,1,0:T(1,128)S(1)}, u32[]{:S(2)}, u32[]{:S(2)}) async-start(f32[16,1,256]{2,1,0:T(1,128)} %broadcast_in_dim.54), calls=%async_computation.1 | async-start | bytes 32768 | tf_op jit(solution)/shard_map/all_to_all | solution.py:38
  182.5 4.4 %all-to-all-done.1 = f32[16,1,256]{2,1,0:T(1,128)S(1)} async-done(((f32[16,1,256]{2,1,0:T(1,128)}), f32[16,1,256]{2,1,0:T(1,128)S(1)}, u32[]{:S(2)}, u32[]{:S(2)}) %all-to-all-start.1) | async-done | bytes 16416 | tf_op jit(solution)/shard_map/all_to_all | solution.py:38
  187.1 2.0 gather_fusion
  189.1 0.2 broadcast_select_fusion.1
  189.3 19.4 %all_to_all.26 = bf16[32,20,128]{2,1,0:T(8,128)(2,1)S(1)} all-to-all(bf16[32,20,128]{2,1,0:T(8,128)(2,1)S(1)} %broadcast_select_fusion.1), channel_id=1, replica_groups=mesh['sp'=32,'tp'=16] {'sp'}, dimensions={0} | all-to-all | bytes 327680 | tf_op jit(solution)/shard_map/all_to_all | solution.py:201
  208.7 0.7 reshape.586
  209.4 37.6 %all-gather.5.cloned.1.call-done = bf16[640,2048]{1,0:T(8,128)(2,1)} async-done(((bf16[640,128]{1,0:T(8,128)(2,1)}), bf16[640,2048]{1,0:T(8,128)(2,1)}) %all-gather.5.cloned.1.call-update) | async-done | bytes 2621456 | tf_op jit(solution)/shard_map/all_gather | solution.py:204
  247.1 2.7 convolution_minimum_fusion
  249.8 0.9 fusion.30
  250.8 0.9 fusion.25
  251.7 2.2 copy.126
  253.9 5.8 %all-to-all-start.3 = ((bf16[16,32,20,128]{3,1,2,0:T(8,128)(2,1)}), bf16[16,32,20,128]{3,1,2,0:T(8,128)(2,1)}, u32[]{:S(2)}, u32[]{:S(2)}) async-start(bf16[16,32,20,128]{3,1,2,0:T(8,128)(2,1)} %bitcast.176), calls=%async_computation.3 | async-start | bytes 5242880 | tf_op jit(solution)/shard_map/all_to_all | solution.py:32
  259.8 0.1 mul.278
  260.1 59.6 %all-to-all-done.3 = bf16[16,32,20,128]{3,1,2,0:T(8,128)(2,1)} async-done(((bf16[16,32,20,128]{3,1,2,0:T(8,128)(2,1)}), bf16[16,32,20,128]{3,1,2,0:T(8,128)(2,1)}, u32[]{:S(2)}, u32[]{:S(2)}) %all-to-all-start.3) | async-done | bytes 2621472 | tf_op jit(solution)/shard_map/all_to_all | solution.py:32
  319.7 2.1 reduce_sum.107
  321.8 0.7 copy.107
  322.6 10.2 %all-to-all-start.4 = ((bf16[32,20,128]{2,1,0:T(8,128)(2,1)}), bf16[32,20,128]{2,1,0:T(8,128)(2,1)S(1)}, u32[]{:S(2)}, u32[]{:S(2)}) async-start(bf16[32,20,128]{2,1,0:T(8,128)(2,1)} %copy.107), calls=%async_computation.4 | async-start | bytes 393216 | tf_op jit(solution)/shard_map/all_to_all | solution.py:212
  332.8 11.8 %all-to-all-done.4 = bf16[32,20,128]{2,1,0:T(8,128)(2,1)S(1)} async-done(((bf16[32,20,128]{2,1,0:T(8,128)(2,1)}), bf16[32,20,128]{2,1,0:T(8,128)(2,1)S(1)}, u32[]{:S(2)}, u32[]{:S(2)}) %all-to-all-start.4) | async-done | bytes 163872 | tf_op jit(solution)/shard_map/all_to_all | solution.py:212
  344.7 1.3 gather_fusion.1
  346.0 0.4 fusion.35
  346.4 0.7 add_convert_fusion
  (93 shorter events, 2.8 us)
Async XLA Ops:
  6.5 244.3 %copy-start = (bf16[1,256,2048]{2,1,0:T(8,128)(2,1)S(1)}, bf16[1,256,2048]{2,1,0:T(8,128)(2,1)}, u32[]{:S(2)}) copy-start(bf16[1,256,2048]{2,1,0:T(8,128)(2,1)} %param.29) | copy-start | bytes 3145732
  6.5 89.9 %all-gather.3.cloned.1.call-start = ((), (), s32[]{:S(2)}) async-start(), calls=%async_computation.5 | async-start | bytes 2297856 | tf_op jit(solution)/shard_map/all_gather | solution.py:17
  105.9 35.1 %copy-start.3 = (bf16[128,2048]{1,0:T(8,128)(2,1)S(1)}, bf16[128,2048]{1,0:T(8,128)(2,1)}, u32[]{:S(2)}) copy-start(bf16[128,2048]{1,0:T(8,128)(2,1)} %param.22) | copy-start | bytes 1572868
  110.0 3.5 copy-start.1
  118.7 3.5 copy-start.1
  127.5 3.5 copy-start.1
  136.2 3.5 copy-start.1
  140.9 9.2 %copy-start.4 = (s32[256,2]{0,1:T(2,128)S(1)}, s32[256,2]{0,1:T(2,128)}, u32[]{:S(2)}) copy-start(s32[256,2]{0,1:T(2,128)} %param.25) | copy-start | bytes 6148
  140.9 35.5 %copy-start.2 = (bf16[256,128]{1,0:T(8,128)(2,1)S(1)}, bf16[256,128]{1,0:T(8,128)(2,1)}, u32[]{:S(2)}) copy-start(bf16[256,128]{1,0:T(8,128)(2,1)} %param.23) | copy-start | bytes 196612
  140.9 46.0 %copy-start.6 = (f32[128]{0:T(128)S(1)}, f32[128]{0:T(128)}, u32[]{:S(2)}) copy-start(f32[128]{0:T(128)} %param.24) | copy-start | bytes 1540
  142.7 104.4 %copy-start.8 = (bf16[1,2048,256]{2,1,0:T(8,128)(2,1)S(1)}, bf16[1,2048,256]{2,1,0:T(8,128)(2,1)}, u32[]{:S(2)}) copy-start(bf16[1,2048,256]{2,1,0:T(8,128)(2,1)} %param.27) | copy-start | bytes 3145732
  142.7 33.6 %all-to-all-start = ((bf16[16,128,256]{1,2,0:T(8,128)(2,1)}), bf16[16,128,256]{1,2,0:T(8,128)(2,1)S(1)}, u32[]{:S(2)}, u32[]{:S(2)}) async-start(bf16[16,128,256]{1,2,0:T(8,128)(2,1)} %bitcast.153), calls=%async_computation | async-start | bytes 2097152 | tf_op jit(solution)/shard_map/all_to_all | solution.py:32
  177.2 9.7 %all-to-all-start.1 = ((f32[16,1,256]{2,1,0:T(1,128)}), f32[16,1,256]{2,1,0:T(1,128)S(1)}, u32[]{:S(2)}, u32[]{:S(2)}) async-start(f32[16,1,256]{2,1,0:T(1,128)} %broadcast_in_dim.54), calls=%async_computation.1 | async-start | bytes 32768 | tf_op jit(solution)/shard_map/all_to_all | solution.py:38
  182.4 64.7 %all-gather.5.cloned.1.call-start = ((), (), s32[]{:S(2)}) async-start(), calls=%async_computation.6 | async-start | bytes 2785280 | tf_op jit(solution)/shard_map/all_gather | solution.py:204
  247.0 2.8 copy-start.7
  247.1 2.8 copy-start.9
  251.7 8.3 %copy-start.5 = (f32[256,2]{0,1:T(2,128)S(1)}, f32[256,2]{0,1:T(2,128)}, u32[]{:S(2)}) copy-start(f32[256,2]{0,1:T(2,128)} %param.26) | copy-start | bytes 6148
  253.9 65.8 %all-to-all-start.3 = ((bf16[16,32,20,128]{3,1,2,0:T(8,128)(2,1)}), bf16[16,32,20,128]{3,1,2,0:T(8,128)(2,1)}, u32[]{:S(2)}, u32[]{:S(2)}) async-start(bf16[16,32,20,128]{3,1,2,0:T(8,128)(2,1)} %bitcast.176), calls=%async_computation.3 | async-start | bytes 5242880 | tf_op jit(solution)/shard_map/all_to_all | solution.py:32
  322.6 22.1 %all-to-all-start.4 = ((bf16[32,20,128]{2,1,0:T(8,128)(2,1)}), bf16[32,20,128]{2,1,0:T(8,128)(2,1)S(1)}, u32[]{:S(2)}, u32[]{:S(2)}) async-start(bf16[32,20,128]{2,1,0:T(8,128)(2,1)} %copy.107), calls=%async_computation.4 | async-start | bytes 393216 | tf_op jit(solution)/shard_map/all_to_all | solution.py:212
Sparse Core Ops, SparseCore 0:
  10.9 85.4 all-gather.2
  209.6 37.4 all-gather.4
where the time goes:
time: 355 us; the launch traced here: 354 us
  waiting for transfers between devices  220 us (62%)
  matrix products  33.4 us (9%)
  starting transfers between devices  28.6 us (8%)
  local copies, waits for them, and re-layouts  22.1 us (6%)
  blocking collectives  19.4 us (5%)
  other arithmetic  16.7 us (5%)
  between operations  13.9 us (4%)
    all_gather x1, waiting for transfers between devices, sent_together(): lax.all_gather(both, axis, axis=dim, tiled=True)  83.1 us
    all_to_all x2, waiting for transfers between devices, summed_on_arrival(): lax.all_to_all(cut_along(value, dim, length), axis, 0, 0, tiled=True)  82.7 us
    all_gather x1, waiting for transfers between devices, per_device(): column_piece = lax.all_gather(flat_rows, 'tp', axis=1, tiled=True)  37.6 us
    all_to_all x1, blocking collectives, per_device(): lax.all_to_all(outgoing, 'sp', split_axis=0, concat_axis=0, tiled=True)  19.4 us
    dot_general x4, matrix products, softmax_update(): jnp.einsum('tkgd,pkd->tkgp', query_rot, key_block, preferred_element_type...  14.5 us
    dot_general x4, matrix products, softmax_update(): jnp.einsum('tkgp,pkd->tkgd', weights.astype(jnp.bfloat16), value_block, p...  13.9 us
    all_to_all x2, starting transfers between devices, summed_on_arrival(): lax.all_to_all(cut_along(value, dim, length), axis, 0, 0, tiled=True)  13.2 us
    all_to_all x1, waiting for transfers between devices, per_device(): lax.all_to_all(expert_out, 'sp', split_axis=0, concat_axis=0, tiled=True)  11.8 us
  transfers between devices with their start and end apart: 6, of which 6 were waited for; matrix products, arithmetic and copies ran while one was open for 2% of the time, Pallas kernels for 0%

commit v1 on v0

--- a/solution.py
+++ b/solution.py
@@ -201,7 +201,10 @@
     arrived = lax.all_to_all(outgoing, "sp", split_axis=0, concat_axis=0, tiled=True)
     sources = arrived.shape[0]
     flat_rows = arrived.reshape(-1, width_local)
-    column_piece = lax.all_gather(flat_rows, "tp", axis=1, tiled=True)
+    peers = lax.axis_size("tp")
+    pieces = jnp.stack([flat_rows for _ in range(peers)])
+    pieces = lax.all_to_all(pieces, "tp", split_axis=0, concat_axis=0)
+    column_piece = jnp.concatenate(pieces, axis=1)
     gate_pre = jnp.dot(column_piece, gate_local, preferred_element_type=jnp.float32)
     up_pre = jnp.dot(column_piece, up_local, preferred_element_type=jnp.float32)
     hidden = clamped_unit(gate_pre, up_pre)

time: 355 us -> 375 us (1.056)
  blocking collectives: 19.4 us -> 85.1 us
  waiting for transfers between devices: 220 us -> 183 us
  starting transfers between devices: 28.6 us -> 21.6 us
    all_to_all x0 -> x1, blocking collectives: none -> 65.6 us  [per_device(): pieces = lax.all_to_all(pieces, 'tp', split_axis=0, concat_axis=0)]
    all_gather x1 -> x0, waiting for transfers between devices: 37.6 us -> none  [per_device(): column_piece = lax.all_gather(flat_rows, 'tp', axis=1, tiled=True)]
    all_to_all x1, starting transfers between devices: 10.2 us -> 3.86 us  [per_device(): lax.all_to_all(expert_out, 'sp', split_axis=0, concat_axis=0, tiled=True)]
  transfers between devices with their start and end apart: 6 -> 5, of which waited for: 6 -> 5; matrix products, arithmetic and copies ran while one was open for 2% -> 2% of each run, Pallas kernels for 0% -> 0%
where the time goes in v1:
time: 375 us; the launch traced here: 374 us
  waiting for transfers between devices  183 us (49%)
  blocking collectives  85.1 us (23%)
  matrix products  31.5 us (8%)
  local copies, waits for them, and re-layouts  22.2 us (6%)
  starting transfers between devices  21.6 us (6%)
  other arithmetic  16.7 us (4%)
  between operations  13.8 us (4%)
    all_gather x1, waiting for transfers between devices, sent_together(): lax.all_gather(both, axis, axis=dim, tiled=True)  83.1 us
    all_to_all x2, waiting for transfers between devices, summed_on_arrival(): lax.all_to_all(cut_along(value, dim, length), axis, 0, 0, tiled=True)  82.7 us
    all_to_all x1, blocking collectives, per_device(): pieces = lax.all_to_all(pieces, 'tp', split_axis=0, concat_axis=0)  65.6 us
    all_to_all x1, blocking collectives, per_device(): lax.all_to_all(outgoing, 'sp', split_axis=0, concat_axis=0, tiled=True)  19.4 us
    dot_general x4, matrix products, softmax_update(): jnp.einsum('tkgd,pkd->tkgp', query_rot, key_block, preferred_element_type...  14.5 us
    dot_general x4, matrix products, softmax_update(): jnp.einsum('tkgp,pkd->tkgd', weights.astype(jnp.bfloat16), value_block, p...  13.9 us
    all_to_all x2, starting transfers between devices, summed_on_arrival(): lax.all_to_all(cut_along(value, dim, length), axis, 0, 0, tiled=True)  12.5 us
    all_to_all x1, waiting for transfers between devices, per_device(): lax.all_to_all(expert_out, 'sp', split_axis=0, concat_axis=0, tiled=True)  12.3 us
  transfers between devices with their start and end apart: 5, of which 5 were waited for; matrix products, arithmetic and copies ran while one was open for 2% of the time, Pallas kernels for 0%

profile of v1, /device:TPU:24, one launch (start us, length us, event | category | flops | bytes accessed | tf_op | source)
XLA Modules:
  0.0 373.7 jit_solution(15596140421105486915)
XLA Ops:
  6.6 0.9 fusion.36
  7.5 0.8 fusion.37
  8.7 0.7 convert_element_type.95
  9.4 1.4 pad_maximum_fusion
  10.8 0.9 copy.97
  11.8 0.8 mul.256
  12.9 0.2 subtract_convert_fusion
  13.1 0.2 pad_maximum_fusion.1
  13.3 83.1 %all-gather.2.cloned.1.call-done = bf16[8192,129]{0,1:T(8,128)(2,1)} async-done(((bf16[256,129]{0,1:T(8,128)(2,1)}), bf16[8192,129]{0,1:T(8,128)(2,1)}) %all-gather.2.cloned.1.call-update) | async-done | bytes 2113552 | tf_op jit(solution)/shard_map/all_gather | solution.py:17
  96.4 2.7 fusion.54
  99.1 1.8 reshape.586
  100.9 1.6 copy.98
  102.5 0.8 reshape.587
  103.3 1.6 copy.99
  104.9 1.0 slice_reduce_fusion.1
  105.9 35.0 %while.15 = (s32[]{:T(128)}, f32[256,1,2]{0,2,1:T(2,128)S(1)}, f32[256,1,2]{0,2,1:T(2,128)S(1)}, f32[256,1,2,64]{0,3,2,1:T(8,128)S(1)}, bf16[256]{0:T(256)(128)(...) while((s32[]{:T(128)}, f32[256,1,2]{0,2,1:T(2,128)S(1)}, ...), condition=%wide.region_5.6_spmd.clone, body=%wide.region_2.5_spmd.clone.sunk | while | flops 282692608 | bytes 32355992 | solution.py:158
  105.9 0.4 broadcast_compare_fusion.3
  106.3 3.6 fusion.68
  110.0 3.5 fusion.71
  113.5 1.1 fusion.70
  114.7 0.4 broadcast_compare_fusion.3
  115.1 3.6 fusion.68
  118.7 3.5 fusion.71
  122.2 1.1 fusion.70
  123.4 0.4 broadcast_compare_fusion.3
  123.8 3.6 fusion.68
  127.5 3.5 fusion.71
  131.0 1.1 fusion.70
  132.2 0.4 broadcast_compare_fusion.3
  132.6 3.6 fusion.68
  136.2 3.5 fusion.71
  139.7 1.1 fusion.70
  141.0 0.5 fusion.26
  141.4 1.3 copy.132
  142.7 7.2 %all-to-all-start = ((bf16[16,128,256]{1,2,0:T(8,128)(2,1)}), bf16[16,128,256]{1,2,0:T(8,128)(2,1)S(1)}, u32[]{:S(2)}, u32[]{:S(2)}) async-start(bf16[16,128,256]{1,2,0:T(8,128)(2,1)} %bitcast.156), calls=%async_computation | async-start | bytes 2097152 | tf_op jit(solution)/shard_map/all_to_all | solution.py:32
  150.4 1.2 reduce-window.6
  151.6 0.2 slice_reduce_fusion
  152.0 0.4 fusion.27
  152.6 0.4 and_reduce_fusion
  153.1 23.1 %all-to-all-done = bf16[16,128,256]{1,2,0:T(8,128)(2,1)S(1)} async-done(((bf16[16,128,256]{1,2,0:T(8,128)(2,1)}), bf16[16,128,256]{1,2,0:T(8,128)(2,1)S(1)}, u32[]{:S(2)}, u32[]{:S(2)}) %all-to-all-start) | async-done | bytes 1048608 | tf_op jit(solution)/shard_map/all_to_all | solution.py:32
  176.4 0.6 broadcast_in_dim.54
  177.0 5.2 %all-to-all-start.1 = ((f32[16,1,256]{2,1,0:T(1,128)}), f32[16,1,256]{2,1,0:T(1,128)S(1)}, u32[]{:S(2)}, u32[]{:S(2)}) async-start(f32[16,1,256]{2,1,0:T(1,128)} %broadcast_in_dim.54), calls=%async_computation.1 | async-start | bytes 32768 | tf_op jit(solution)/shard_map/all_to_all | solution.py:38
  182.4 4.4 %all-to-all-done.1 = f32[16,1,256]{2,1,0:T(1,128)S(1)} async-done(((f32[16,1,256]{2,1,0:T(1,128)}), f32[16,1,256]{2,1,0:T(1,128)S(1)}, u32[]{:S(2)}, u32[]{:S(2)}) %all-to-all-start.1) | async-done | bytes 16416 | tf_op jit(solution)/shard_map/all_to_all | solution.py:38
  186.9 2.0 gather_fusion
  189.0 0.2 broadcast_select_fusion.1
  189.1 19.4 %all_to_all.31 = bf16[32,20,128]{2,1,0:T(8,128)(2,1)S(1)} all-to-all(bf16[32,20,128]{2,1,0:T(8,128)(2,1)S(1)} %broadcast_select_fusion.1), channel_id=1, replica_groups=mesh['sp'=32,'tp'=16] {'sp'}, dimensions={0} | all-to-all | bytes 327680 | tf_op jit(solution)/shard_map/all_to_all | solution.py:201
  208.6 0.2 copy.108
  208.8 0.3 stack.17
  209.1 65.6 %all_to_all.32 = bf16[16,640,128]{1,2,0:T(8,128)(2,1)S(1)} all-to-all(bf16[16,640,128]{1,2,0:T(8,128)(2,1)S(1)} %stack.17), channel_id=1, replica_groups=mesh['sp'=32,'tp'=16] {'tp'}, dimensions={0} | all-to-all | bytes 5242880 | tf_op jit(solution)/shard_map/all_to_all | solution.py:206
  274.7 0.9 convolution_minimum_fusion
  275.6 0.3 copy-done.8
  276.0 0.9 fusion.30
  277.0 0.9 fusion.25
  277.8 2.2 copy.131
  280.0 5.3 %all-to-all-start.4 = ((bf16[16,32,20,128]{3,1,2,0:T(8,128)(2,1)}), bf16[16,32,20,128]{3,1,2,0:T(8,128)(2,1)}, u32[]{:S(2)}, u32[]{:S(2)}) async-start(bf16[16,32,20,128]{3,1,2,0:T(8,128)(2,1)} %bitcast.179), calls=%async_computation.4 | async-start | bytes 5242880 | tf_op jit(solution)/shard_map/all_to_all | solution.py:32
  285.5 0.1 mul.278
  285.8 59.6 %all-to-all-done.4 = bf16[16,32,20,128]{3,1,2,0:T(8,128)(2,1)} async-done(((bf16[16,32,20,128]{3,1,2,0:T(8,128)(2,1)}), bf16[16,32,20,128]{3,1,2,0:T(8,128)(2,1)}, u32[]{:S(2)}, u32[]{:S(2)}) %all-to-all-start.4) | async-done | bytes 2621472 | tf_op jit(solution)/shard_map/all_to_all | solution.py:32
  345.4 2.1 reduce_sum.107
  347.5 0.7 copy.112
  348.2 3.9 %all-to-all-start.5 = ((bf16[32,20,128]{2,1,0:T(8,128)(2,1)}), bf16[32,20,128]{2,1,0:T(8,128)(2,1)S(1)}, u32[]{:S(2)}, u32[]{:S(2)}) async-start(bf16[32,20,128]{2,1,0:T(8,128)(2,1)} %copy.112), calls=%async_computation.5 | async-start | bytes 393216 | tf_op jit(solution)/shard_map/all_to_all | solution.py:215
  352.1 12.3 %all-to-all-done.5 = bf16[32,20,128]{2,1,0:T(8,128)(2,1)S(1)} async-done(((bf16[32,20,128]{2,1,0:T(8,128)(2,1)}), bf16[32,20,128]{2,1,0:T(8,128)(2,1)S(1)}, u32[]{:S(2)}, u32[]{:S(2)}) %all-to-all-start.5) | async-done | bytes 163872 | tf_op jit(solution)/shard_map/all_to_all | solution.py:215
  364.5 1.3 gather_fusion.1
  365.8 0.4 fusion.35
  366.2 0.7 add_convert_fusion
  (91 shorter events, 3.1 us)
Async XLA Ops:
  6.5 270.4 %copy-start = (bf16[1,256,2048]{2,1,0:T(8,128)(2,1)S(1)}, bf16[1,256,2048]{2,1,0:T(8,128)(2,1)}, u32[]{:S(2)}) copy-start(bf16[1,256,2048]{2,1,0:T(8,128)(2,1)} %param.29) | copy-start | bytes 3145732
  6.5 89.9 %all-gather.2.cloned.1.call-start = ((), (), s32[]{:S(2)}) async-start(), calls=%async_computation.6 | async-start | bytes 2297856 | tf_op jit(solution)/shard_map/all_gather | solution.py:17
  105.9 35.1 %copy-start.3 = (bf16[128,2048]{1,0:T(8,128)(2,1)S(1)}, bf16[128,2048]{1,0:T(8,128)(2,1)}, u32[]{:S(2)}) copy-start(bf16[128,2048]{1,0:T(8,128)(2,1)} %param.22) | copy-start | bytes 1572868
  110.0 3.5 copy-start.1
  118.7 3.5 copy-start.1
  127.5 3.5 copy-start.1
  136.2 3.5 copy-start.1
  140.9 9.0 %copy-start.4 = (s32[256,2]{0,1:T(2,128)S(1)}, s32[256,2]{0,1:T(2,128)}, u32[]{:S(2)}) copy-start(s32[256,2]{0,1:T(2,128)} %param.25) | copy-start | bytes 6148
  140.9 35.4 %copy-start.2 = (bf16[256,128]{1,0:T(8,128)(2,1)S(1)}, bf16[256,128]{1,0:T(8,128)(2,1)}, u32[]{:S(2)}) copy-start(bf16[256,128]{1,0:T(8,128)(2,1)} %param.23) | copy-start | bytes 196612
  140.9 45.9 %copy-start.6 = (f32[128]{0:T(128)S(1)}, f32[128]{0:T(128)}, u32[]{:S(2)}) copy-start(f32[128]{0:T(128)} %param.24) | copy-start | bytes 1540
  142.7 33.5 %all-to-all-start = ((bf16[16,128,256]{1,2,0:T(8,128)(2,1)}), bf16[16,128,256]{1,2,0:T(8,128)(2,1)S(1)}, u32[]{:S(2)}, u32[]{:S(2)}) async-start(bf16[16,128,256]{1,2,0:T(8,128)(2,1)} %bitcast.156), calls=%async_computation | async-start | bytes 2097152 | tf_op jit(solution)/shard_map/all_to_all | solution.py:32
  177.0 9.7 %all-to-all-start.1 = ((f32[16,1,256]{2,1,0:T(1,128)}), f32[16,1,256]{2,1,0:T(1,128)S(1)}, u32[]{:S(2)}, u32[]{:S(2)}) async-start(f32[16,1,256]{2,1,0:T(1,128)} %broadcast_in_dim.54), calls=%async_computation.1 | async-start | bytes 32768 | tf_op jit(solution)/shard_map/all_to_all | solution.py:38
  208.6 66.1 %copy-start.7 = (bf16[1,2048,256]{2,1,0:T(8,128)(2,1)S(1)}, bf16[1,2048,256]{2,1,0:T(8,128)(2,1)}, u32[]{:S(2)}) copy-start(bf16[1,2048,256]{2,1,0:T(8,128)(2,1)} %param.27) | copy-start | bytes 3145732
  274.7 1.2 copy-start.8
  277.8 7.8 %copy-start.5 = (f32[256,2]{0,1:T(2,128)S(1)}, f32[256,2]{0,1:T(2,128)}, u32[]{:S(2)}) copy-start(f32[256,2]{0,1:T(2,128)} %param.26) | copy-start | bytes 6148
  280.0 65.3 %all-to-all-start.4 = ((bf16[16,32,20,128]{3,1,2,0:T(8,128)(2,1)}), bf16[16,32,20,128]{3,1,2,0:T(8,128)(2,1)}, u32[]{:S(2)}, u32[]{:S(2)}) async-start(bf16[16,32,20,128]{3,1,2,0:T(8,128)(2,1)} %bitcast.179), calls=%async_computation.4 | async-start | bytes 5242880 | tf_op jit(solution)/shard_map/all_to_all | solution.py:32
  348.2 16.2 %all-to-all-start.5 = ((bf16[32,20,128]{2,1,0:T(8,128)(2,1)}), bf16[32,20,128]{2,1,0:T(8,128)(2,1)S(1)}, u32[]{:S(2)}, u32[]{:S(2)}) async-start(bf16[32,20,128]{2,1,0:T(8,128)(2,1)} %copy.112), calls=%async_computation.5 | async-start | bytes 393216 | tf_op jit(solution)/shard_map/all_to_all | solution.py:215
Sparse Core Ops, SparseCore 0:
  10.9 85.4 all-gather.1
